TPU v7x, 32 devices: a whole 2x2x4 slice. The times are simulated.
32 devices in a mesh: sp: 8 (over z, x), dp: 4 (over y, core).
Axes of the slice: x: 2, y: 2, z: 4, core: 2. Of those that a mesh axis runs over, the one named last changes fastest.
Arguments:
- gate_in: bfloat16 [4, 4096, 1024], P('dp', 'sp'), may hold values from -6 to 6
- value_in: bfloat16 [4, 4096, 1024], P('dp', 'sp'), may hold values from -6 to 6
- segments: int32 [4, 4096], P('dp', 'sp'), may hold values from 0 to 1, never falling along the last dimension, each value on 1 to 3072 neighbouring positions
- value_gain: bfloat16 [1024], P('sp'), may hold values from 0.099609375 to 1.8984375
- mixing: bfloat16 [8, 1024, 1024], P('sp', 'dp'), may hold values from -0.1875 to 0.1875
- mixing_bias: bfloat16 [8, 1024], P('sp'), may hold values from 0.099609375 to 1.8984375
Outputs:
- gated: bfloat16 [4, 4096, 1024], P('dp', 'sp')
Inputs may be any that keep to these rules, and one draw needn't show every extreme that they name: `segments`: within each sequence the numbers never fall, every number 0 to 1 occurs, a document spans at most 3072 positions and some document spans exactly that.
All inputs are finite; a program needn't handle non-finite values.
Results may differ from a plain program's by a relative error of at most 0.0054.
Values may be sent and summed in bfloat16 or wider, within the bound.
No kernel may reach another device: no remote copies, remote signals or barrier semaphores. Data moves between devices by JAX's collectives and lax.ppermute only.
A program may use at most 128 MiB of HBM per device.

v0:
```python
import jax
import jax.numpy as jnp
from jax import lax
from jax.sharding import PartitionSpec as P

HEAD_DIM = 128
epsilon = 1e-06


def head_norm(values, gain_f, head_dim):
    shaped = values.reshape(values.shape[:-1] + (values.shape[-1] // head_dim, head_dim))
    scaled = shaped * lax.rsqrt(jnp.mean(shaped * shaped, axis=-1, keepdims=True) + epsilon)
    return (scaled.reshape(values.shape) * gain_f).astype(jnp.bfloat16)


def per_device(gate_in, value_in, segments, value_gain, mixing, mixing_bias):
    sp_count = lax.axis_size("sp")
    sequences = value_in.shape[0]
    tokens = value_in.shape[1]
    length = tokens * sp_count
    block_len = mixing.shape[2]
    heads_here = mixing.shape[0]
    head_dim = HEAD_DIM
    id_tile = jnp.broadcast_to(
        segments.astype(jnp.bfloat16)[:, :, None], (sequences, tokens, sp_count)
    )
    value_heads, id_heads = (
        lax.all_to_all(value_in, "sp", split_axis=2, concat_axis=1, tiled=True),
        lax.all_to_all(id_tile, "sp", split_axis=2, concat_axis=1, tiled=True),
    )
    gain_f = value_gain.astype(jnp.float32)
    normed = head_norm(jax.nn.gelu(value_heads.astype(jnp.float32)), gain_f, head_dim)
    blocks = sequences * length // block_len
    value_blocks = normed.reshape(blocks, block_len, heads_here, head_dim)
    id_blocks = id_heads.reshape(blocks, block_len)
    bias_f = mixing_bias.astype(jnp.float32)
    nothing = jnp.zeros((), jnp.bfloat16)
    shard_piece = lax.all_gather(mixing, "dp", axis=1, tiled=True)
    bias_rows = jnp.transpose(bias_f)[:, :, None]

    def one_block(pair_item):
        block_values, block_ids = pair_item
        same_doc = block_ids[:, None] == block_ids[None, :]
        masked = jnp.where(same_doc[None, :, :], shard_piece, nothing)
        summed = jnp.einsum(
            "hts,shd->thd", masked, block_values, preferred_element_type=jnp.float32
        )
        return (summed + bias_rows).astype(jnp.bfloat16)

    mixed = lax.map(one_block, (value_blocks, id_blocks))
    mixed = mixed.reshape(sequences, length, heads_here * head_dim)
    returned = lax.all_to_all(mixed, "sp", split_axis=1, concat_axis=2, tiled=True)
    return (jax.nn.gelu(gate_in.astype(jnp.float32)) * returned.astype(jnp.float32)).astype(
        jnp.bfloat16
    )


def solution(mesh):
    return jax.shard_map(
        per_device,
        mesh=mesh,
        in_specs=(
            P("dp", "sp", None),
            P("dp", "sp", None),
            P("dp", "sp"),
            P("sp"),
            P("sp", "dp", None),
            P("sp", None),
        ),
        out_specs=P("dp", "sp", None),
        check_vma=False,
    )
```

profile of v0, /device:TPU:0, one launch (start us, length us, event | category | flops | bytes accessed | tf_op | source)
XLA Modules:
  0.0 162.7 jit_solution(6695371021300023633)
XLA Ops:
  6.5 0.0 all-gather.2.cloned.1.call-start
  6.5 0.7 all-gather.2.cloned.1.call-update
  7.3 0.7 convert_reduce_fusion
  8.0 0.5 broadcast.193
  8.5 0.6 reduce.7
  9.0 0.6 reshape.283
  9.7 7.3 %all-to-all-start.1 = ((bf16[8,2,256]{2,1,0:T(2,128)(2,1)}), bf16[8,2,256]{2,1,0:T(2,128)(2,1)S(1)}, u32[]{:S(2)}, u32[]{:S(2)}) async-start(bf16[8,2,256]{2,1,0:T(2,128)(2,1)} %reshape.283), calls=%async_computation.1 | async-start | bytes 16384 | tf_op jit(solution)/shard_map/all_to_all | solution.py:29
  16.9 4.7 %copy.44 = bf16[1,512,1024]{1,0,2:T(2,128)(2,1)S(1)} copy(bf16[1,512,1024]{2,1,0:T(8,128)(2,1)} %param.9) | data formatting | bytes 2097152 | tf_op args[1]
  21.6 6.9 %reduce.6 = bf16[1024,512]{1,0:T(8,128)(2,1)S(1)} reduce(bf16[1024,1,512]{2,1,0:T(2,128)(2,1)S(1)} %bitcast.83, bf16[]{:T(256)} %broadcast.193), dimensions={1}, to_apply=%bitcast.59.reduce_sub_computation | reduce | bytes 2097154
  28.6 0.0 copy-start.4
  28.6 0.0 copy-start.3
  28.6 1.6 reshape.281
  30.2 0.0 all-to-all-done.1
  30.2 6.0 %all-to-all-start = ((bf16[8,2,32768]{2,1,0:T(2,128)(2,1)}), bf16[8,2,32768]{2,1,0:T(2,128)(2,1)S(1)}, u32[]{:S(2)}, u32[]{:S(2)}) async-start(bf16[8,2,32768]{2,1,0:T(2,128)(2,1)} %reshape.281), calls=%async_computation | async-start | bytes 2097152 | tf_op jit(solution)/shard_map/all_to_all | solution.py:28
  36.2 0.0 copy-done.4
  36.2 0.0 copy-done.3
  36.3 25.3 %all-to-all-done = bf16[8,2,32768]{2,1,0:T(2,128)(2,1)S(1)} async-done(((bf16[8,2,32768]{2,1,0:T(2,128)(2,1)}), bf16[8,2,32768]{2,1,0:T(2,128)(2,1)S(1)}, u32[]{:S(2)}, u32[]{:S(2)}) %all-to-all-start) | async-done | bytes 1048608 | tf_op jit(solution)/shard_map/all_to_all | solution.py:28
  61.6 1.0 reshape.282
  62.6 0.3 copy.45
  62.9 0.5 copy.46
  63.5 0.8 fusion.47
  64.3 0.0 copy-start.1
  64.4 1.7 %fusion.31 = bf16[4,1024,1,128]{3,1,2,0:T(8,128)(2,1)} fusion(f32[4,1024,1,128]{3,1,2,0:T(8,128)S(1)} %bitcast.79, f32[128]{0:T(128)S(1)} %convert_element_type.89, f32[4,1024]{1,0:T(4,128)S(1)} %rsqrt.12), kind=kLoop, calls=%fused_computation.31 | loop fusion | flops 5767168 | bytes 3162624 | tf_op jit(solution)/shard_map/convert_element_type | solution.py:13
  66.0 0.0 all-gather.2.cloned.1.call-done
  66.0 0.0 copy-done.1
  66.0 11.5 %while.10 = (s32[]{:T(128)}, bf16[4,1024,1,128]{3,1,0,2:T(8,128)(2,1)S(1)}, bf16[4,1024,1,128]{3,1,2,0:T(8,128)(2,1)}, bf16[4,1024]{1,0:T(4,128)(2,1)S(1)}, bf16...) while((s32[]{:T(128)}, bf16[4,1024,1,128]{3,1,0,2:T(8,128)(2,1)S(1)}, ...), condition=%wide.region_2.3_spmd, body=%wide.region_1.2_spmd.sunk | while | flops 270794752 | bytes 3682901 | solution.py:50
  66.1 2.6 %fusion.53 = bf16[1,1024,1,128]{1,3,2,0:T(8,128)(2,1)S(1)} fusion(bf16[1,1024,1024]{2,1,0:T(8,128)(2,1)} %get-tuple-element.105, bf16[1024]{0:T(1024)(128)(2,1)S(1)} %dynamic-slice_reduce_fusion.2, f32[1024]{0:T(1024)S(1)} %bitcast.89, bf16[4,1024,1,128]{3,1,2,0:T(8,128)(2,1)} %get-tuple-element.103, s32[]{:T(128)} %get-tuple-element.94), kind=kOutput, calls=%fused_computation.6.clone.1 | convolution fusion | flops 270794752 | bytes 2630144 | tf_op jit(solution)/shard_map/while/body/eval_jaxpr/hts,shd->thd/dot_general | solution.py:45
  68.7 0.2 copy.65
  69.0 2.6 %fusion.53 = bf16[1,1024,1,128]{1,3,2,0:T(8,128)(2,1)S(1)} fusion(bf16[1,1024,1024]{2,1,0:T(8,128)(2,1)} %get-tuple-element.105, bf16[1024]{0:T(1024)(128)(2,1)S(1)} %dynamic-slice_reduce_fusion.2, f32[1024]{0:T(1024)S(1)} %bitcast.89, bf16[4,1024,1,128]{3,1,2,0:T(8,128)(2,1)} %get-tuple-element.103, s32[]{:T(128)} %get-tuple-element.94), kind=kOutput, calls=%fused_computation.6.clone.1 | convolution fusion | flops 270794752 | bytes 2630144 | tf_op jit(solution)/shard_map/while/body/eval_jaxpr/hts,shd->thd/dot_general | solution.py:45
  71.6 0.2 copy.65
  71.8 2.6 %fusion.53 = bf16[1,1024,1,128]{1,3,2,0:T(8,128)(2,1)S(1)} fusion(bf16[1,1024,1024]{2,1,0:T(8,128)(2,1)} %get-tuple-element.105, bf16[1024]{0:T(1024)(128)(2,1)S(1)} %dynamic-slice_reduce_fusion.2, f32[1024]{0:T(1024)S(1)} %bitcast.89, bf16[4,1024,1,128]{3,1,2,0:T(8,128)(2,1)} %get-tuple-element.103, s32[]{:T(128)} %get-tuple-element.94), kind=kOutput, calls=%fused_computation.6.clone.1 | convolution fusion | flops 270794752 | bytes 2630144 | tf_op jit(solution)/shard_map/while/body/eval_jaxpr/hts,shd->thd/dot_general | solution.py:45
  74.5 0.2 copy.65
  74.7 2.6 %fusion.53 = bf16[1,1024,1,128]{1,3,2,0:T(8,128)(2,1)S(1)} fusion(bf16[1,1024,1024]{2,1,0:T(8,128)(2,1)} %get-tuple-element.105, bf16[1024]{0:T(1024)(128)(2,1)S(1)} %dynamic-slice_reduce_fusion.2, f32[1024]{0:T(1024)S(1)} %bitcast.89, bf16[4,1024,1,128]{3,1,2,0:T(8,128)(2,1)} %get-tuple-element.103, s32[]{:T(128)} %get-tuple-element.94), kind=kOutput, calls=%fused_computation.6.clone.1 | convolution fusion | flops 270794752 | bytes 2630144 | tf_op jit(solution)/shard_map/while/body/eval_jaxpr/hts,shd->thd/dot_general | solution.py:45
  77.3 0.2 copy.65
  77.6 16.7 %copy.63 = bf16[1,4096,128]{2,0,1:T(2,128)(2,1)S(1)} copy(bf16[1,4096,128]{2,1,0:T(8,128)(2,1)S(1)} %bitcast.86) | data formatting | bytes 2097152 | tf_op jit(solution)/shard_map/reshape | solution.py:51
  94.3 22.3 %reduce.8 = bf16[4096,128]{1,0:T(8,128)(2,1)S(1)} reduce(bf16[4096,1,128]{2,1,0:T(2,128)(2,1)S(1)} %bitcast.82, bf16[]{:T(256)} %broadcast.193), dimensions={1}, to_apply=%bitcast.68.reduce_sub_computation | reduce | bytes 2097154
  116.6 0.0 copy-start.2
  116.6 1.1 reshape.285
  117.7 3.6 %all-to-all-start.2 = ((bf16[8,2,32768]{2,1,0:T(2,128)(2,1)}), bf16[8,2,32768]{2,1,0:T(2,128)(2,1)S(1)}, u32[]{:S(2)}, u32[]{:S(2)}) async-start(bf16[8,2,32768]{2,1,0:T(2,128)(2,1)} %reshape.285), calls=%async_computation.2 | async-start | bytes 2097152 | tf_op jit(solution)/shard_map/all_to_all | solution.py:52
  121.3 0.0 copy-done.2
  121.3 1.3 copy.43
  122.6 24.4 %all-to-all-done.2 = bf16[8,2,32768]{2,1,0:T(2,128)(2,1)S(1)} async-done(((bf16[8,2,32768]{2,1,0:T(2,128)(2,1)}), bf16[8,2,32768]{2,1,0:T(2,128)(2,1)S(1)}, u32[]{:S(2)}, u32[]{:S(2)}) %all-to-all-start.2) | async-done | bytes 1048608 | tf_op jit(solution)/shard_map/all_to_all | solution.py:52
  147.1 1.0 reshape.286
  148.1 0.1 copy.54
  148.3 1.5 convert_bitcast_fusion
  149.8 0.0 copy-start
  149.8 2.0 %copy.55 = f32[1,512,8,128]{1,3,2,0:T(8,128)S(1)} copy(f32[1,512,8,128]{3,1,2,0:T(8,128)} %convert_bitcast_fusion) | data formatting | bytes 4194304 | tf_op jit(solution)/shard_map/convert_element_type | solution.py:53
  151.8 0.0 copy-done
  151.8 1.8 %fusion.46 = bf16[1,512,1024]{1,2,0:T(8,128)(2,1)} fusion(bf16[1,512,1024]{1,2,0:T(8,128)(2,1)S(1)} %copy-done, f32[1,512,8,128]{1,3,2,0:T(8,128)S(1)} %copy.55), kind=kLoop, calls=%fused_computation.46 | loop fusion | flops 5767168 | bytes 4194304 | tf_op jit(solution)/shard_map/convert_element_type | solution.py:53
  153.6 2.3 %copy.56 = bf16[1,512,1024]{2,1,0:T(8,128)(2,1)} copy(bf16[1,512,1024]{1,2,0:T(8,128)(2,1)} %fusion.46) | data formatting | bytes 2097152 | tf_op jit(solution)/shard_map/convert_element_type | solution.py:53
  (17 shorter events, 0.3 us)
Async XLA Ops:
  6.5 59.5 %all-gather.2.cloned.1.call-start = ((), (), s32[]{:S(2)}) async-start(), calls=%async_computation.3 | async-start | bytes 2621440 | tf_op jit(solution)/shard_map/all_gather | solution.py:38
  9.7 20.5 %all-to-all-start.1 = ((bf16[8,2,256]{2,1,0:T(2,128)(2,1)}), bf16[8,2,256]{2,1,0:T(2,128)(2,1)S(1)}, u32[]{:S(2)}, u32[]{:S(2)}) async-start(bf16[8,2,256]{2,1,0:T(2,128)(2,1)} %reshape.283), calls=%async_computation.1 | async-start | bytes 16384 | tf_op jit(solution)/shard_map/all_to_all | solution.py:29
  28.6 7.6 %copy-start.4 = (bf16[128]{0:T(256)(128)(2,1)S(1)}, bf16[128]{0:T(256)(128)(2,1)}, u32[]{:S(2)}) copy-start(bf16[128]{0:T(256)(128)(2,1)} %param.11) | copy-start | bytes 772
  28.6 7.6 %copy-start.3 = (bf16[1,1024]{1,0:T(2,128)(2,1)S(1)}, bf16[1,1024]{1,0:T(2,128)(2,1)}, u32[]{:S(2)}) copy-start(bf16[1,1024]{1,0:T(2,128)(2,1)} %param.13) | copy-start | bytes 6148
  30.2 31.4 %all-to-all-start = ((bf16[8,2,32768]{2,1,0:T(2,128)(2,1)}), bf16[8,2,32768]{2,1,0:T(2,128)(2,1)S(1)}, u32[]{:S(2)}, u32[]{:S(2)}) async-start(bf16[8,2,32768]{2,1,0:T(2,128)(2,1)} %reshape.281), calls=%async_computation | async-start | bytes 2097152 | tf_op jit(solution)/shard_map/all_to_all | solution.py:28
  64.3 1.7 %copy-start.1 = (bf16[4,1024,1,128]{3,1,0,2:T(8,128)(2,1)S(1)}, bf16[4,1024,1,128]{3,1,0,2:T(8,128)(2,1)}, u32[]{:S(2)}) copy-start(bf16[4,1024,1,128]{3,1,0,2:T(8,128)(2,1)} %custom-call) | copy-start | bytes 3145732
  116.6 4.7 %copy-start.2 = (bf16[1,512,1024]{2,1,0:T(8,128)(2,1)S(1)}, bf16[1,512,1024]{2,1,0:T(8,128)(2,1)}, u32[]{:S(2)}) copy-start(bf16[1,512,1024]{2,1,0:T(8,128)(2,1)} %param.8) | copy-start | bytes 3145732
  117.7 29.3 %all-to-all-start.2 = ((bf16[8,2,32768]{2,1,0:T(2,128)(2,1)}), bf16[8,2,32768]{2,1,0:T(2,128)(2,1)S(1)}, u32[]{:S(2)}, u32[]{:S(2)}) async-start(bf16[8,2,32768]{2,1,0:T(2,128)(2,1)} %reshape.285), calls=%async_computation.2 | async-start | bytes 2097152 | tf_op jit(solution)/shard_map/all_to_all | solution.py:52
  149.8 2.0 %copy-start = (bf16[1,512,1024]{1,2,0:T(8,128)(2,1)S(1)}, bf16[1,512,1024]{1,2,0:T(8,128)(2,1)}, u32[]{:S(2)}) copy-start(bf16[1,512,1024]{1,2,0:T(8,128)(2,1)} %copy.43) | copy-start | bytes 3145732
Sparse Core Ops, SparseCore 0:
  8.9 25.2 all-gather.1
where the time goes:
time: 163 us
  waiting for transfers between devices  50.5 us (31%)
  other arithmetic  36.3 us (22%)
  local copies, waits for them, and re-layouts  34.9 us (21%)
  starting transfers between devices  16.8 us (10%)
  between operations  13.6 us (8%)
  matrix products  10.4 us (6%)
    unnamed x3, other arithmetic  29.8 us
    all_to_all x1, waiting for transfers between devices, per_device(): lax.all_to_all(value_in, 'sp', split_axis=2, concat_axis=1, tiled=True)  25.3 us
    all_to_all x1, waiting for transfers between devices, per_device(): lax.all_to_all(mixed, 'sp', split_axis=1, concat_axis=2, tiled=True)  24.4 us
    reshape x1, local copies, waits for them, and re-layouts, per_device(): mixed = mixed.reshape(sequences, length, heads_here * head_dim)  16.7 us
    unnamed x21, local copies, waits for them, and re-layouts  11.9 us
    dot_general x4, matrix products, one_block(): jnp.einsum('hts,shd->thd', masked, block_values, preferred_element_type=j...  10.4 us
    all_to_all x1, starting transfers between devices, per_device(): lax.all_to_all(id_tile, 'sp', split_axis=2, concat_axis=1, tiled=True)  7.28 us
    all_to_all x1, starting transfers between devices, per_device(): lax.all_to_all(value_in, 'sp', split_axis=2, concat_axis=1, tiled=True)  5.99 us
  transfers between devices with their start and end apart: 4, of which 2 were waited for; matrix products, arithmetic and copies ran while one was open for 13% of the time, Pallas kernels for 0%

commit v1 on v0

--- a/solution.py
+++ b/solution.py
@@ -49,7 +49,9 @@
 
     mixed = lax.map(one_block, (value_blocks, id_blocks))
     mixed = mixed.reshape(sequences, length, heads_here * head_dim)
-    returned = lax.all_to_all(mixed, "sp", split_axis=1, concat_axis=2, tiled=True)
+    returned = jnp.concatenate(
+        lax.all_to_all(jnp.stack(jnp.split(mixed, lax.axis_size("sp"), axis=1)), "sp", 0, 0), axis=2
+    )
     return (jax.nn.gelu(gate_in.astype(jnp.float32)) * returned.astype(jnp.float32)).astype(
         jnp.bfloat16
     )

time: 163 us -> 127 us (0.78)
  other arithmetic: 36.3 us -> 14.2 us
  local copies, waits for them, and re-layouts: 34.9 us -> 20.3 us
    unnamed x3 -> x2, other arithmetic: 29.8 us -> 7.68 us
    reshape x1 -> x0, local copies, waits for them, and re-layouts: 16.7 us -> none  [per_device(): mixed = mixed.reshape(sequences, length, heads_here * head_dim)]
    unnamed x21 -> x24, local copies, waits for them, and re-layouts: 11.9 us -> 13.7 us
  transfers between devices with their start and end apart: 4 -> 4, of which waited for: 2 -> 2; matrix products, arithmetic and copies ran while one was open for 13% -> 16% of each run, Pallas kernels for 0% -> 0%
where the time goes in v1:
time: 127 us
  waiting for transfers between devices  51.2 us (40%)
  local copies, waits for them, and re-layouts  20.3 us (16%)
  starting transfers between devices  16.8 us (13%)
  other arithmetic  14.2 us (11%)
  between operations  13.6 us (11%)
  matrix products  10.4 us (8%)
    all_to_all x1, waiting for transfers between devices, per_device(): lax.all_to_all(value_in, 'sp', split_axis=2, concat_axis=1, tiled=True)  25.3 us
    all_to_all x1, waiting for transfers between devices, per_device(): lax.all_to_all(jnp.stack(jnp.split(mixed, lax.axis_size('sp'), axis=1)),...  25.2 us
    unnamed x24, local copies, waits for them, and re-layouts  13.7 us
    dot_general x4, matrix products, one_block(): jnp.einsum('hts,shd->thd', masked, block_values, preferred_element_type=j...  10.4 us
    unnamed x2, other arithmetic  7.68 us
    all_to_all x1, starting transfers between devices, per_device(): lax.all_to_all(id_tile, 'sp', split_axis=2, concat_axis=1, tiled=True)  7.28 us
    all_to_all x1, starting transfers between devices, per_device(): lax.all_to_all(value_in, 'sp', split_axis=2, concat_axis=1, tiled=True)  5.99 us
    all_to_all x1, starting transfers between devices, per_device(): lax.all_to_all(jnp.stack(jnp.split(mixed, lax.axis_size('sp'), axis=1)),...  3.56 us
  transfers between devices with their start and end apart: 4, of which 2 were waited for; matrix products, arithmetic and copies ran while one was open for 16% of the time, Pallas kernels for 0%

profile of v1, /device:TPU:0, one launch (start us, length us, event | category | flops | bytes accessed | tf_op | source)
XLA Modules:
  0.0 126.7 jit_solution(86155714421104263)
XLA Ops:
  6.5 0.0 all-gather.2.cloned.1.call-start
  6.5 0.7 all-gather.2.cloned.1.call-update
  7.3 0.7 convert_reduce_fusion
  8.0 0.5 broadcast.193
  8.5 0.7 reduce.7
  9.2 0.6 reshape.282
  9.8 7.3 %all-to-all-start.1 = ((bf16[8,2,256]{2,1,0:T(2,128)(2,1)}), bf16[8,2,256]{2,1,0:T(2,128)(2,1)S(1)}, u32[]{:S(2)}, u32[]{:S(2)}) async-start(bf16[8,2,256]{2,1,0:T(2,128)(2,1)} %reshape.282), calls=%async_computation.1 | async-start | bytes 16384 | tf_op jit(solution)/shard_map/all_to_all | solution.py:29
  17.1 4.7 %copy.45 = bf16[1,512,1024]{1,0,2:T(2,128)(2,1)S(1)} copy(bf16[1,512,1024]{2,1,0:T(8,128)(2,1)} %param.9) | data formatting | bytes 2097152 | tf_op args[1]
  21.7 7.0 %reduce.6 = bf16[1024,512]{1,0:T(8,128)(2,1)S(1)} reduce(bf16[1024,1,512]{2,1,0:T(2,128)(2,1)S(1)} %bitcast.107, bf16[]{:T(256)} %broadcast.193), dimensions={1}, to_apply=%bitcast.89.reduce_sub_computation | reduce | bytes 2097154
  28.7 0.0 copy-start.3
  28.8 0.0 copy-start.2
  28.8 1.6 %reshape.280 = bf16[8,2,32768]{2,1,0:T(2,128)(2,1)} reshape(bf16[1024,512]{1,0:T(8,128)(2,1)S(1)} %reduce.6) | data formatting | bytes 2097152
  30.4 0.0 all-to-all-done.1
  30.4 6.0 %all-to-all-start = ((bf16[8,2,32768]{2,1,0:T(2,128)(2,1)}), bf16[8,2,32768]{2,1,0:T(2,128)(2,1)S(1)}, u32[]{:S(2)}, u32[]{:S(2)}) async-start(bf16[8,2,32768]{2,1,0:T(2,128)(2,1)} %reshape.280), calls=%async_computation | async-start | bytes 2097152 | tf_op jit(solution)/shard_map/all_to_all | solution.py:28
  36.4 0.0 copy-done.3
  36.4 0.0 copy-done.2
  36.5 25.3 %all-to-all-done = bf16[8,2,32768]{2,1,0:T(2,128)(2,1)S(1)} async-done(((bf16[8,2,32768]{2,1,0:T(2,128)(2,1)}), bf16[8,2,32768]{2,1,0:T(2,128)(2,1)S(1)}, u32[]{:S(2)}, u32[]{:S(2)}) %all-to-all-start) | async-done | bytes 1048608 | tf_op jit(solution)/shard_map/all_to_all | solution.py:28
  61.8 1.0 reshape.281
  62.8 0.3 copy.46
  63.1 0.5 copy.47
  63.6 0.8 fusion.47
  64.5 0.0 copy-start
  64.5 1.7 %fusion.31 = bf16[4,1024,1,128]{3,1,2,0:T(8,128)(2,1)} fusion(f32[4,1024,1,128]{3,1,2,0:T(8,128)S(1)} %bitcast.105, f32[128]{0:T(128)S(1)} %convert_element_type.86, f32[4,1024]{1,0:T(4,128)S(1)} %rsqrt.12), kind=kLoop, calls=%fused_computation.31 | loop fusion | flops 5767168 | bytes 3162624 | tf_op jit(solution)/shard_map/convert_element_type | solution.py:13
  66.2 0.0 all-gather.2.cloned.1.call-done
  66.2 0.0 copy-done
  66.2 11.5 %while.10 = (s32[]{:T(128)}, bf16[4,1024,1,128]{3,1,0,2:T(8,128)(2,1)S(1)}, bf16[4,1024,1,128]{3,1,2,0:T(8,128)(2,1)}, bf16[4,1024]{1,0:T(4,128)(2,1)S(1)}, bf16...) while((s32[]{:T(128)}, bf16[4,1024,1,128]{3,1,0,2:T(8,128)(2,1)S(1)}, ...), condition=%wide.region_2.3_spmd, body=%wide.region_1.2_spmd.sunk | while | flops 270794752 | bytes 3682901 | solution.py:50
  66.2 2.6 %fusion.61 = bf16[1,1024,1,128]{1,3,2,0:T(8,128)(2,1)S(1)} fusion(bf16[1,1024,1024]{2,1,0:T(8,128)(2,1)} %get-tuple-element.105, bf16[1024]{0:T(1024)(128)(2,1)S(1)} %dynamic-slice_reduce_fusion.2, f32[1024]{0:T(1024)S(1)} %bitcast.119, bf16[4,1024,1,128]{3,1,2,0:T(8,128)(2,1)} %get-tuple-element.103, s32[]{:T(128)} %get-tuple-element.94), kind=kOutput, calls=%fused_computation.6.clone.1 | convolution fusion | flops 270794752 | bytes 2630144 | tf_op jit(solution)/shard_map/while/body/eval_jaxpr/hts,shd->thd/dot_general | solution.py:45
  68.9 0.2 copy.62
  69.1 2.6 %fusion.61 = bf16[1,1024,1,128]{1,3,2,0:T(8,128)(2,1)S(1)} fusion(bf16[1,1024,1024]{2,1,0:T(8,128)(2,1)} %get-tuple-element.105, bf16[1024]{0:T(1024)(128)(2,1)S(1)} %dynamic-slice_reduce_fusion.2, f32[1024]{0:T(1024)S(1)} %bitcast.119, bf16[4,1024,1,128]{3,1,2,0:T(8,128)(2,1)} %get-tuple-element.103, s32[]{:T(128)} %get-tuple-element.94), kind=kOutput, calls=%fused_computation.6.clone.1 | convolution fusion | flops 270794752 | bytes 2630144 | tf_op jit(solution)/shard_map/while/body/eval_jaxpr/hts,shd->thd/dot_general | solution.py:45
  71.7 0.2 copy.62
  72.0 2.6 %fusion.61 = bf16[1,1024,1,128]{1,3,2,0:T(8,128)(2,1)S(1)} fusion(bf16[1,1024,1024]{2,1,0:T(8,128)(2,1)} %get-tuple-element.105, bf16[1024]{0:T(1024)(128)(2,1)S(1)} %dynamic-slice_reduce_fusion.2, f32[1024]{0:T(1024)S(1)} %bitcast.119, bf16[4,1024,1,128]{3,1,2,0:T(8,128)(2,1)} %get-tuple-element.103, s32[]{:T(128)} %get-tuple-element.94), kind=kOutput, calls=%fused_computation.6.clone.1 | convolution fusion | flops 270794752 | bytes 2630144 | tf_op jit(solution)/shard_map/while/body/eval_jaxpr/hts,shd->thd/dot_general | solution.py:45
  74.6 0.2 copy.62
  74.9 2.6 %fusion.61 = bf16[1,1024,1,128]{1,3,2,0:T(8,128)(2,1)S(1)} fusion(bf16[1,1024,1024]{2,1,0:T(8,128)(2,1)} %get-tuple-element.105, bf16[1024]{0:T(1024)(128)(2,1)S(1)} %dynamic-slice_reduce_fusion.2, f32[1024]{0:T(1024)S(1)} %bitcast.119, bf16[4,1024,1,128]{3,1,2,0:T(8,128)(2,1)} %get-tuple-element.103, s32[]{:T(128)} %get-tuple-element.94), kind=kOutput, calls=%fused_computation.6.clone.1 | convolution fusion | flops 270794752 | bytes 2630144 | tf_op jit(solution)/shard_map/while/body/eval_jaxpr/hts,shd->thd/dot_general | solution.py:45
  77.5 0.2 copy.62
  77.7 0.0 copy-start.1
  77.7 0.7 fusion.55
  78.4 0.7 fusion.54
  79.1 0.7 fusion.53
  79.7 0.7 fusion.52
  80.4 0.7 fusion.51
  81.1 0.7 fusion.50
  81.7 0.7 fusion.49
  82.4 0.7 fusion.48
  83.1 3.6 %all-to-all-start.2 = ((bf16[8,1,512,128]{3,2,1,0:T(8,128)(2,1)}), bf16[8,1,512,128]{3,2,1,0:T(8,128)(2,1)S(1)}, u32[]{:S(2)}, u32[]{:S(2)}) async-start(bf16[8,1,512,128]{3,2,1,0:T(8,128)(2,1)} %fusion.48), calls=%async_computation.2 | async-start | bytes 2097152 | tf_op jit(solution)/shard_map/all_to_all | solution.py:53
  86.6 0.0 copy-done.1
  86.6 0.5 copy.44
  87.2 25.2 %all-to-all-done.2 = bf16[8,1,512,128]{3,2,1,0:T(8,128)(2,1)S(1)} async-done(((bf16[8,1,512,128]{3,2,1,0:T(8,128)(2,1)}), bf16[8,1,512,128]{3,2,1,0:T(8,128)(2,1)S(1)}, u32[]{:S(2)}, u32[]{:S(2)}) %all-to-all-start.2) | async-done | bytes 1048608 | tf_op jit(solution)/shard_map/all_to_all | solution.py:53
  112.4 1.5 %convert_bitcast_fusion = f32[1,512,8,128]{3,1,0,2:T(8,128)} fusion(bf16[8,1,512,128]{3,2,1,0:T(8,128)(2,1)S(1)} %all-to-all-done.2), kind=kLoop, calls=%fused_computation.47 | loop fusion | flops 524288 | bytes 3145728 | tf_op jit(solution)/shard_map/convert_element_type | solution.py:55
  113.9 1.9 %copy.54 = f32[1,512,8,128]{1,3,2,0:T(8,128)S(1)} copy(f32[1,512,8,128]{3,1,0,2:T(8,128)} %convert_bitcast_fusion) | data formatting | bytes 4194304 | tf_op jit(solution)/shard_map/convert_element_type | solution.py:55
  115.8 1.8 %fusion.46 = bf16[1,512,1024]{1,2,0:T(8,128)(2,1)} fusion(bf16[1,512,1024]{1,2,0:T(8,128)(2,1)S(1)} %copy.44, f32[1,512,8,128]{1,3,2,0:T(8,128)S(1)} %copy.54), kind=kLoop, calls=%fused_computation.46 | loop fusion | flops 5767168 | bytes 4194304 | tf_op jit(solution)/shard_map/convert_element_type | solution.py:55
  117.6 2.3 %copy.55 = bf16[1,512,1024]{2,1,0:T(8,128)(2,1)} copy(bf16[1,512,1024]{1,2,0:T(8,128)(2,1)} %fusion.46) | data formatting | bytes 2097152 | tf_op jit(solution)/shard_map/convert_element_type | solution.py:55
  (17 shorter events, 0.3 us)
Async XLA Ops:
  6.5 59.7 %all-gather.2.cloned.1.call-start = ((), (), s32[]{:S(2)}) async-start(), calls=%async_computation.3 | async-start | bytes 2621440 | tf_op jit(solution)/shard_map/all_gather | solution.py:38
  9.8 20.6 %all-to-all-start.1 = ((bf16[8,2,256]{2,1,0:T(2,128)(2,1)}), bf16[8,2,256]{2,1,0:T(2,128)(2,1)S(1)}, u32[]{:S(2)}, u32[]{:S(2)}) async-start(bf16[8,2,256]{2,1,0:T(2,128)(2,1)} %reshape.282), calls=%async_computation.1 | async-start | bytes 16384 | tf_op jit(solution)/shard_map/all_to_all | solution.py:29
  28.7 7.6 %copy-start.3 = (bf16[128]{0:T(256)(128)(2,1)S(1)}, bf16[128]{0:T(256)(128)(2,1)}, u32[]{:S(2)}) copy-start(bf16[128]{0:T(256)(128)(2,1)} %param.11) | copy-start | bytes 772
  28.8 7.6 %copy-start.2 = (bf16[1,1024]{1,0:T(2,128)(2,1)S(1)}, bf16[1,1024]{1,0:T(2,128)(2,1)}, u32[]{:S(2)}) copy-start(bf16[1,1024]{1,0:T(2,128)(2,1)} %param.13) | copy-start | bytes 6148
  30.4 31.4 %all-to-all-start = ((bf16[8,2,32768]{2,1,0:T(2,128)(2,1)}), bf16[8,2,32768]{2,1,0:T(2,128)(2,1)S(1)}, u32[]{:S(2)}, u32[]{:S(2)}) async-start(bf16[8,2,32768]{2,1,0:T(2,128)(2,1)} %reshape.280), calls=%async_computation | async-start | bytes 2097152 | tf_op jit(solution)/shard_map/all_to_all | solution.py:28
  64.5 1.7 %copy-start = (bf16[4,1024,1,128]{3,1,0,2:T(8,128)(2,1)S(1)}, bf16[4,1024,1,128]{3,1,0,2:T(8,128)(2,1)}, u32[]{:S(2)}) copy-start(bf16[4,1024,1,128]{3,1,0,2:T(8,128)(2,1)} %custom-call.1) | copy-start | bytes 3145732
  77.7 8.9 %copy-start.1 = (bf16[1,512,1024]{2,1,0:T(8,128)(2,1)S(1)}, bf16[1,512,1024]{2,1,0:T(8,128)(2,1)}, u32[]{:S(2)}) copy-start(bf16[1,512,1024]{2,1,0:T(8,128)(2,1)} %param.8) | copy-start | bytes 3145732
  83.1 29.3 %all-to-all-start.2 = ((bf16[8,1,512,128]{3,2,1,0:T(8,128)(2,1)}), bf16[8,1,512,128]{3,2,1,0:T(8,128)(2,1)S(1)}, u32[]{:S(2)}, u32[]{:S(2)}) async-start(bf16[8,1,512,128]{3,2,1,0:T(8,128)(2,1)} %fusion.48), calls=%async_computation.2 | async-start | bytes 2097152 | tf_op jit(solution)/shard_map/all_to_all | solution.py:53
Sparse Core Ops, SparseCore 0:
  8.9 25.2 all-gather.1
